TPU v7x, 512 devices: a 8x2x16 block of a 8x8x16 slice. The times are simulated.
512 devices in a mesh: grp: 2 (over y), sp: 16 (over z), dp: 16 (over x, core).
Axes of the slice: x: 8, y: 2, z: 16, core: 2. Of those that a mesh axis runs over, the one named last changes fastest.
The devices are a block of a 8x8x16 slice.
Arguments:
- query_rows: bfloat16 [32, 2048, 2048], P(('grp', 'dp'), 'sp'), parts along dimension 0, may hold values from -6 to 6
- key_rows: bfloat16 [32, 2048, 2048], P(('grp', 'dp'), 'sp'), parts along dimension 0, may hold values from -6 to 6
- value_rows: bfloat16 [32, 2048, 2048], P(('grp', 'dp'), 'sp'), parts along dimension 0, may hold values from -6 to 6
- query_gain: float32 [64], replicated, may hold values from 1.1 to 7
- key_gain: float32 [64], replicated, may hold values from 1.1 to 7
- lambdas: float32 [16], replicated, may hold values from 0.3 to 0.8
- head_gain: float32 [128], replicated, may hold values from 0.1 to 1.9
- out_weight: bfloat16 [2048, 2048], P(None, 'dp'), may hold values from -0.125 to 0.125
Outputs:
- attended: bfloat16 [32, 2048, 2048], P(('grp', 'dp'), 'sp'), parts along dimension 0
There are 2 independent parts, one for each index of `grp`. A program takes and returns all parts, laid end to end along the dimension named above; an argument that names none is the same for every part. Nothing has to cross between parts.
All inputs are finite; a program needn't handle non-finite values.
Results may differ from a plain program's by a relative error of at most 0.008.
The roundings to bfloat16 on the way count: a program that leaves them out, or rounds other values in their place, can miss the bound.
Values may be sent and summed in bfloat16 or wider, within the bound.
A program may use at most 128 MiB of HBM per device.

v0:
```python
import jax
import jax.numpy as jnp
from jax import lax
from jax.sharding import PartitionSpec as P

EPSILON = 1e-06
OUT_SCALE = 0.8


def in_one_piece(arrays, axis, split_dim, concat_dim, along):
    ends, at = ([], 0)
    for a in arrays[:-1]:
        at += a.shape[along]
        ends.append(at)
    both = jnp.concatenate(arrays, axis=along)
    return tuple(
        jnp.split(
            lax.all_to_all(both, axis, split_axis=split_dim, concat_axis=concat_dim, tiled=True),
            ends,
            axis=along,
        )
    )


def split_up(array, dim, count):
    before, after = (array.shape[:dim], array.shape[dim + 1 :])
    return jnp.moveaxis(array.reshape(*before, count, -1, *after), dim, 0)


def edges_of(length, count):
    step = length // count
    if step >= 8:
        step -= step % 8
    return [step * k for k in range(1, count)]


def laid_out(pieces, dim):
    pieces = jnp.moveaxis(pieces, 0, dim)
    shape = pieces.shape
    return pieces.reshape(*shape[:dim], shape[dim] * shape[dim + 1], *shape[dim + 2 :])


def several_exchanges(array, axis, pieces, split_dim, concat_dim):
    blocks = split_up(array, split_dim, lax.axis_size(axis))
    split_at = max(range(1, max(2, blocks.ndim - 1)), key=lambda d: blocks.shape[d])
    outs = []
    for section in jnp.split(blocks, edges_of(blocks.shape[split_at], pieces), axis=split_at):
        if section.size:
            outs.append(lax.all_to_all(section, axis, split_axis=0, concat_axis=0, tiled=True))
    return laid_out(jnp.concatenate(outs, axis=split_at), concat_dim)


def norm_rotate(field_rows, gain_vector, positions):
    widened = field_rows.astype(jnp.float32)
    normed = (
        widened
        * lax.rsqrt(jnp.mean(widened * widened, axis=-1, keepdims=True) + EPSILON)
        * gain_vector
    )
    half_size = field_rows.shape[-1] // 2
    inverse = 10000.0 ** (-jnp.arange(half_size, dtype=jnp.float32) / half_size)
    angles = (positions[:, None] * inverse[None, :]).reshape(positions.shape[0], 1, 1, half_size)
    cosine_part = jnp.cos(angles)
    sine_part = jnp.sin(angles)
    first_half = normed[..., :half_size]
    second_half = normed[..., half_size:]
    turned = jnp.concatenate(
        [
            first_half * cosine_part - second_half * sine_part,
            second_half * cosine_part + first_half * sine_part,
        ],
        axis=-1,
    )
    return turned.astype(jnp.bfloat16)


def head_norm(raw_heads, gain_vector):
    scaled = raw_heads * lax.rsqrt(
        jnp.mean(raw_heads * raw_heads, axis=-1, keepdims=True) + EPSILON
    )
    return (scaled * gain_vector * OUT_SCALE).astype(jnp.bfloat16)


def block_size():
    return 512


def attend(query_head, key_head, value_head, weight_two, gain_vector):
    length = query_head.shape[0]
    block_rows = block_size()
    score_scale = query_head.shape[-1] ** (-0.5)
    offsets = jnp.arange(block_rows, dtype=jnp.int32)
    value_size = value_head.shape[-1]

    def one_block(number):
        first_row = number * block_rows
        query_block = lax.dynamic_slice_in_dim(query_head, first_row, block_rows, 0)
        query_positions = first_row + offsets

        def fill_scores(kblock, buffer):
            key_block = lax.dynamic_slice_in_dim(key_head, kblock * block_rows, block_rows, 0)
            scores = (
                jnp.einsum(
                    "qcd,kcd->cqk", query_block, key_block, preferred_element_type=jnp.float32
                )
                * score_scale
            )
            visible = (kblock * block_rows + offsets)[None, :] <= query_positions[:, None]
            scores = jnp.where(visible[None], scores, -1e30)
            return lax.dynamic_update_slice_in_dim(buffer, scores, kblock * block_rows, 2)

        start_buffer = jnp.full((2, block_rows, length), -1e30, jnp.float32)
        stored = lax.fori_loop(0, number + 1, fill_scores, start_buffer)
        highest = jnp.max(stored, axis=-1)
        totals = jnp.sum(jnp.exp(stored - highest[..., None]), axis=-1)

        def weigh_values(kblock, accumulated):
            scores = lax.dynamic_slice_in_dim(stored, kblock * block_rows, block_rows, 2)
            probabilities = jnp.exp(scores - highest[..., None]) / totals[..., None]
            mixing = (probabilities[0] - weight_two * probabilities[1]).astype(jnp.bfloat16)
            value_block = lax.dynamic_slice_in_dim(value_head, kblock * block_rows, block_rows, 0)
            return accumulated + jnp.dot(mixing, value_block, preferred_element_type=jnp.float32)

        return lax.fori_loop(
            0, number + 1, weigh_values, jnp.zeros((block_rows, value_size), jnp.float32)
        )

    blocks = lax.map(one_block, jnp.arange(length // block_rows, dtype=jnp.int32))
    return head_norm(blocks.reshape(length, value_size), gain_vector)


def local(query_rows, key_rows, value_rows, query_gain, key_gain, lambdas, head_gain, out_weight):
    tok_count = query_rows.shape[1]
    group_size = lax.axis_size("sp")
    head_size = query_gain.shape[0]
    value_size = head_gain.shape[0]
    heads_total = lambdas.shape[0]
    local_heads = heads_total // group_size

    def by_peer(tensor):
        return tensor.reshape(1, tok_count, group_size, tensor.shape[2] // group_size)

    query_in, key_in, value_in = in_one_piece(
        (by_peer(query_rows), by_peer(key_rows), by_peer(value_rows)), "sp", 2, 1, 0
    )
    length = tok_count * group_size
    positions = jnp.arange(length, dtype=jnp.float32)
    query_rot = norm_rotate(
        query_in.reshape(length, local_heads, 2, head_size), query_gain, positions
    )
    key_rot = norm_rotate(key_in.reshape(length, local_heads, 2, head_size), key_gain, positions)
    value_heads = value_in.reshape(length, local_heads, value_size)
    local_lambdas = lax.dynamic_slice_in_dim(
        lambdas, lax.axis_index("sp") * local_heads, local_heads
    )

    def per_head(head_index):
        return attend(
            query_rot[:, head_index],
            key_rot[:, head_index],
            value_heads[:, head_index],
            local_lambdas[head_index],
            head_gain,
        )

    outputs = lax.map(per_head, jnp.arange(local_heads, dtype=jnp.int32))
    outputs = jnp.transpose(outputs, (1, 0, 2)).reshape(1, length, 1, local_heads * value_size)
    returned = several_exchanges(outputs, "sp", 2, 1, 2)
    heads_rows = returned.reshape(tok_count, heads_total * value_size)
    attended = jnp.dot(
        heads_rows,
        lax.all_gather(out_weight, "dp", axis=1, tiled=True),
        preferred_element_type=jnp.float32,
    )
    return attended.astype(jnp.bfloat16).reshape(1, tok_count, attended.shape[1])


def solution(mesh):
    placed = (
        P(("grp", "dp"), "sp", None),
        P(("grp", "dp"), "sp", None),
        P(("grp", "dp"), "sp", None),
        P(),
        P(),
        P(),
        P(),
        P(None, "dp"),
    )
    return jax.shard_map(
        local, mesh=mesh, in_specs=placed, out_specs=P(("grp", "dp"), "sp", None), check_vma=False
    )
```

profile of v0, /device:TPU:82, one launch (start us, length us, event | category | flops | bytes accessed | tf_op | source)
XLA Modules:
  0.0 363.5 jit_solution(3135334128520861951)
XLA Ops:
  11.3 43.8 %all-to-all-start = ((bf16[3,128,16,128]{3,1,0,2:T(8,128)(2,1)}), bf16[3,128,16,128]{3,1,0,2:T(8,128)(2,1)S(1)}, u32[]{:S(2)}, u32[]{:S(2)}) async-start(bf16[3,128,16,128]{3,1,0,2:T(8,128)(2,1)} %copy.88), calls=%async_computation | async-start | bytes 3145728 | tf_op jit(solution)/shard_map/all_to_all | solution.py:18
  58.4 70.9 %all-to-all-done = bf16[3,128,16,128]{3,1,0,2:T(8,128)(2,1)S(1)} async-done(((bf16[3,128,16,128]{3,1,0,2:T(8,128)(2,1)}), bf16[3,128,16,128]{3,1,0,2:T(8,128)(2,1)S(1)}, u32[]{:S(2)}, u32[]{:S(2)}) %all-to-all-start) | async-done | bytes 1572896 | tf_op jit(solution)/shard_map/all_to_all | solution.py:18
  140.6 157.2 %while.45 = (s32[]{:T(128)}, f32[4,512,128]{2,1,0:T(8,128)}, s32[4]{0:T(128)S(1)}, bf16[2048,2,64]{0,2,1:T(8,128)(2,1)S(1)}, bf16[2048,2,64]{0,2,1:T(8,128)(2,1)...) while((s32[]{:T(128)}, f32[4,512,128]{2,1,0:T(8,128)}, ...), condition=%wide.region_9.10_spmd.clone.clone, body=%wide.region_2.9_spmd.clone.clone.sunk | while | flops 143719456 | bytes 44468540 | solution.py:128
  142.6 4.3 %broadcast.224 = f32[2,512,2048]{1,2,0:T(8,128)} broadcast(f32[]{:T(128)} %constant.21.clone.3..sunk), dimensions={} | broadcast | bytes 8388612 | tf_op jit(solution)/shard_map/broadcast.13
  149.9 3.9 %reduce_max.12 = f32[2,512]{1,0:T(2,128)S(1)} reduce(f32[2,512,2048]{1,2,0:T(8,128)} %get-tuple-element.554, f32[]{:T(128)} %constant.30.clone.3..sunk), dimensions={2}, to_apply=%region_5.5 | reduce | flops 2096128 | bytes 8392708 | tf_op jit(solution)/shard_map/while/body/eval_jaxpr/while/body/eval_jaxpr/reduce_max | solution.py:114
  153.8 4.5 %exponential_reduce_fusion.2 = f32[2,512]{1,0:T(2,128)S(1)} fusion(f32[2,512,2048]{1,2,0:T(8,128)} %get-tuple-element.554, f32[2,512]{1,0:T(2,128)S(1)} %reduce_max.12), kind=kLoop, calls=%fused_computation.17.clone.1 | loop fusion | flops 4193280 | bytes 8396800 | tf_op jit(solution)/shard_map/while/body/eval_jaxpr/while/body/eval_jaxpr/reduce_sum | solution.py:115
  158.3 6.5 %while.47 = (s32[]{:T(128)}, f32[512,128]{1,0:T(8,128)S(1)}, s32[]{:T(128)}, f32[2,512,2048]{1,2,0:T(8,128)}, f32[2,512]{1,0:T(2,128)S(1)}, /*index=5*/f32[2,512...) while((s32[]{:T(128)}, f32[512,128]{1,0:T(8,128)S(1)}, ...), condition=%wide.region_8.8_spmd, body=%wide.region_7.7_spmd.sunk | while | flops 69009416 | bytes 15343791 | solution.py:124
  158.4 3.1 constant_dynamic-slice_fusion.5
  167.5 4.3 %broadcast.224 = f32[2,512,2048]{1,2,0:T(8,128)} broadcast(f32[]{:T(128)} %constant.21.clone.3..sunk), dimensions={} | broadcast | bytes 8388612 | tf_op jit(solution)/shard_map/broadcast.13
  171.8 6.1 %while.46 = (s32[]{:T(128)}, f32[2,512,2048]{1,2,0:T(8,128)}, s32[]{:T(128)}, s32[512]{0:T(512)S(1)}, s32[512]{0:T(512)S(1)}, /*index=5*/bf16[2048,2,64]{0,2,1:T...) while((s32[]{:T(128)}, f32[2,512,2048]{1,2,0:T(8,128)}, ...), condition=%wide.region_4.4_spmd, body=%wide.region_3.3_spmd.sunk | while | flops 68420104 | bytes 2892959 | solution.py:113
  177.9 3.9 %reduce_max.12 = f32[2,512]{1,0:T(2,128)S(1)} reduce(f32[2,512,2048]{1,2,0:T(8,128)} %get-tuple-element.554, f32[]{:T(128)} %constant.30.clone.3..sunk), dimensions={2}, to_apply=%region_5.5 | reduce | flops 2096128 | bytes 8392708 | tf_op jit(solution)/shard_map/while/body/eval_jaxpr/while/body/eval_jaxpr/reduce_max | solution.py:114
  181.8 4.5 %exponential_reduce_fusion.2 = f32[2,512]{1,0:T(2,128)S(1)} fusion(f32[2,512,2048]{1,2,0:T(8,128)} %get-tuple-element.554, f32[2,512]{1,0:T(2,128)S(1)} %reduce_max.12), kind=kLoop, calls=%fused_computation.17.clone.1 | loop fusion | flops 4193280 | bytes 8396800 | tf_op jit(solution)/shard_map/while/body/eval_jaxpr/while/body/eval_jaxpr/reduce_sum | solution.py:115
  186.3 13.1 %while.47 = (s32[]{:T(128)}, f32[512,128]{1,0:T(8,128)S(1)}, s32[]{:T(128)}, f32[2,512,2048]{1,2,0:T(8,128)}, f32[2,512]{1,0:T(2,128)S(1)}, /*index=5*/f32[2,512...) while((s32[]{:T(128)}, f32[512,128]{1,0:T(8,128)S(1)}, ...), condition=%wide.region_8.8_spmd, body=%wide.region_7.7_spmd.sunk | while | flops 69009416 | bytes 15343791 | solution.py:124
  186.3 3.1 constant_dynamic-slice_fusion.5
  192.9 3.1 constant_dynamic-slice_fusion.5
  202.1 4.3 %broadcast.224 = f32[2,512,2048]{1,2,0:T(8,128)} broadcast(f32[]{:T(128)} %constant.21.clone.3..sunk), dimensions={} | broadcast | bytes 8388612 | tf_op jit(solution)/shard_map/broadcast.13
  206.4 9.1 %while.46 = (s32[]{:T(128)}, f32[2,512,2048]{1,2,0:T(8,128)}, s32[]{:T(128)}, s32[512]{0:T(512)S(1)}, s32[512]{0:T(512)S(1)}, /*index=5*/bf16[2048,2,64]{0,2,1:T...) while((s32[]{:T(128)}, f32[2,512,2048]{1,2,0:T(8,128)}, ...), condition=%wide.region_4.4_spmd, body=%wide.region_3.3_spmd.sunk | while | flops 68420104 | bytes 2892959 | solution.py:113
  215.5 3.9 %reduce_max.12 = f32[2,512]{1,0:T(2,128)S(1)} reduce(f32[2,512,2048]{1,2,0:T(8,128)} %get-tuple-element.554, f32[]{:T(128)} %constant.30.clone.3..sunk), dimensions={2}, to_apply=%region_5.5 | reduce | flops 2096128 | bytes 8392708 | tf_op jit(solution)/shard_map/while/body/eval_jaxpr/while/body/eval_jaxpr/reduce_max | solution.py:114
  219.4 4.5 %exponential_reduce_fusion.2 = f32[2,512]{1,0:T(2,128)S(1)} fusion(f32[2,512,2048]{1,2,0:T(8,128)} %get-tuple-element.554, f32[2,512]{1,0:T(2,128)S(1)} %reduce_max.12), kind=kLoop, calls=%fused_computation.17.clone.1 | loop fusion | flops 4193280 | bytes 8396800 | tf_op jit(solution)/shard_map/while/body/eval_jaxpr/while/body/eval_jaxpr/reduce_sum | solution.py:115
  223.9 19.6 %while.47 = (s32[]{:T(128)}, f32[512,128]{1,0:T(8,128)S(1)}, s32[]{:T(128)}, f32[2,512,2048]{1,2,0:T(8,128)}, f32[2,512]{1,0:T(2,128)S(1)}, /*index=5*/f32[2,512...) while((s32[]{:T(128)}, f32[512,128]{1,0:T(8,128)S(1)}, ...), condition=%wide.region_8.8_spmd, body=%wide.region_7.7_spmd.sunk | while | flops 69009416 | bytes 15343791 | solution.py:124
  223.9 3.1 constant_dynamic-slice_fusion.5
  230.4 3.1 constant_dynamic-slice_fusion.5
  237.0 3.1 constant_dynamic-slice_fusion.5
  246.2 4.3 %broadcast.224 = f32[2,512,2048]{1,2,0:T(8,128)} broadcast(f32[]{:T(128)} %constant.21.clone.3..sunk), dimensions={} | broadcast | bytes 8388612 | tf_op jit(solution)/shard_map/broadcast.13
  250.4 12.1 %while.46 = (s32[]{:T(128)}, f32[2,512,2048]{1,2,0:T(8,128)}, s32[]{:T(128)}, s32[512]{0:T(512)S(1)}, s32[512]{0:T(512)S(1)}, /*index=5*/bf16[2048,2,64]{0,2,1:T...) while((s32[]{:T(128)}, f32[2,512,2048]{1,2,0:T(8,128)}, ...), condition=%wide.region_4.4_spmd, body=%wide.region_3.3_spmd.sunk | while | flops 68420104 | bytes 2892959 | solution.py:113
  262.5 3.9 %reduce_max.12 = f32[2,512]{1,0:T(2,128)S(1)} reduce(f32[2,512,2048]{1,2,0:T(8,128)} %get-tuple-element.554, f32[]{:T(128)} %constant.30.clone.3..sunk), dimensions={2}, to_apply=%region_5.5 | reduce | flops 2096128 | bytes 8392708 | tf_op jit(solution)/shard_map/while/body/eval_jaxpr/while/body/eval_jaxpr/reduce_max | solution.py:114
  266.4 4.5 %exponential_reduce_fusion.2 = f32[2,512]{1,0:T(2,128)S(1)} fusion(f32[2,512,2048]{1,2,0:T(8,128)} %get-tuple-element.554, f32[2,512]{1,0:T(2,128)S(1)} %reduce_max.12), kind=kLoop, calls=%fused_computation.17.clone.1 | loop fusion | flops 4193280 | bytes 8396800 | tf_op jit(solution)/shard_map/while/body/eval_jaxpr/while/body/eval_jaxpr/reduce_sum | solution.py:115
  271.0 26.1 %while.47 = (s32[]{:T(128)}, f32[512,128]{1,0:T(8,128)S(1)}, s32[]{:T(128)}, f32[2,512,2048]{1,2,0:T(8,128)}, f32[2,512]{1,0:T(2,128)S(1)}, /*index=5*/f32[2,512...) while((s32[]{:T(128)}, f32[512,128]{1,0:T(8,128)S(1)}, ...), condition=%wide.region_8.8_spmd, body=%wide.region_7.7_spmd.sunk | while | flops 69009416 | bytes 15343791 | solution.py:124
  301.8 24.3 %all_to_all.25 = bf16[16,1,64,1,128]{4,2,3,1,0:T(8,128)(2,1)S(1)} all-to-all(bf16[16,1,64,1,128]{4,2,3,1,0:T(8,128)(2,1)S(1)} %get-tuple-element.336), channel_id=1, replica_groups=mesh['grp'=2,'sp'=16,'dp'=16] {'sp'}, dimensions={0} | all-to-all | bytes 524288 | tf_op jit(solution)/shard_map/all_to_all | solution.py:49
  326.1 6.2 %all-to-all-start.2 = ((bf16[16,1,64,1,128]{4,2,3,1,0:T(8,128)(2,1)}), bf16[16,1,64,1,128]{4,2,3,1,0:T(8,128)(2,1)S(1)}, u32[]{:S(2)}, u32[]{:S(2)}) async-start(bf16[16,1,64,1,128]{4,2,3,1,0:T(8,128)(2,1)} %get-tuple-element.337), calls=%async_computation.2 | async-start | bytes 524288 | tf_op jit(solution)/shard_map/all_to_all | solution.py:49
  332.5 18.0 %all-to-all-done.2 = bf16[16,1,64,1,128]{4,2,3,1,0:T(8,128)(2,1)S(1)} async-done(((bf16[16,1,64,1,128]{4,2,3,1,0:T(8,128)(2,1)}), bf16[16,1,64,1,128]{4,2,3,1,0:T(8,128)(2,1)S(1)}, u32[]{:S(2)}, u32[]{:S(2)}) %all-to-all-start.2) | async-done | bytes 262176 | tf_op jit(solution)/shard_map/all_to_all | solution.py:49
  351.2 5.5 %fusion.12 = bf16[1,128,2048]{2,1,0:T(8,128)(2,1)} fusion(bf16[128,2048]{0,1:T(8,128)(2,1)S(1)} %bitcast.60, bf16[2048,2048]{1,0:T(8,128)(2,1)} %all-gather.2.cloned.1.call-done), kind=kOutput, calls=%fused_computation.22 | convolution fusion | flops 1074003968 | bytes 9437184 | tf_op jit(solution)/shard_map/dot_general | solution.py:170
  (136 shorter events, 109.0 us)
Async XLA Ops:
  6.5 2.7 copy-start.1
  11.3 44.6 %copy-start.5 = (f32[16]{0:T(128)S(1)}, f32[16]{0:T(128)}, u32[]{:S(2)}) copy-start(f32[16]{0:T(128)} %param.19) | copy-start | bytes 196
  11.3 117.9 %all-to-all-start = ((bf16[3,128,16,128]{3,1,0,2:T(8,128)(2,1)}), bf16[3,128,16,128]{3,1,0,2:T(8,128)(2,1)S(1)}, u32[]{:S(2)}, u32[]{:S(2)}) async-start(bf16[3,128,16,128]{3,1,0,2:T(8,128)(2,1)} %copy.88), calls=%async_computation | async-start | bytes 3145728 | tf_op jit(solution)/shard_map/all_to_all | solution.py:18
  55.2 296.0 %all-gather.2.cloned.1.call-start = ((), (), s32[]{:S(2)}) async-start(), calls=%async_computation.3 | async-start | bytes 8912896 | tf_op jit(solution)/shard_map/all_gather | solution.py:172
  132.7 2.2 copy-start.2
  133.6 2.3 copy-start.3
  134.9 1.8 copy-start
  140.6 158.9 %copy-start.4 = (f32[128]{0:T(128)S(1)}, f32[128]{0:T(128)}, u32[]{:S(2)}) copy-start(f32[128]{0:T(128)} %param.20) | copy-start | bytes 1540
  326.1 24.5 %all-to-all-start.2 = ((bf16[16,1,64,1,128]{4,2,3,1,0:T(8,128)(2,1)}), bf16[16,1,64,1,128]{4,2,3,1,0:T(8,128)(2,1)S(1)}, u32[]{:S(2)}, u32[]{:S(2)}) async-start(bf16[16,1,64,1,128]{4,2,3,1,0:T(8,128)(2,1)} %get-tuple-element.337), calls=%async_computation.2 | async-start | bytes 524288 | tf_op jit(solution)/shard_map/all_to_all | solution.py:49
Sparse Core Ops, SparseCore 0:
  58.0 70.5 all-gather.1
where the time goes:
time: 365 us; the launch traced here: 363 us
  waiting for transfers between devices  89.7 us (25%)
  local copies, waits for them, and re-layouts  82.5 us (23%)
  other arithmetic  54.4 us (15%)
  starting transfers between devices  50 us (14%)
  matrix products  43.1 us (12%)
  blocking collectives  24.3 us (7%)
  between operations  13.7 us (4%)
  loops' own time  5.8 us (2%)
    all_to_all x1, waiting for transfers between devices, in_one_piece(): lax.all_to_all(both, axis, split_axis=split_dim, concat_axis=concat_dim,...  70.9 us
    dynamic_slice x20, local copies, waits for them, and re-layouts, weigh_values(): lax.dynamic_slice_in_dim(stored, kblock * block_rows, block_rows, 2)  50.4 us
    all_to_all x1, starting transfers between devices, in_one_piece(): lax.all_to_all(both, axis, split_axis=split_dim, concat_axis=concat_dim,...  43.8 us
    dot_general x10, matrix products, fill_scores(): jnp.einsum('qcd,kcd->cqk', query_block, key_block, preferred_element_type...  28 us
    all_to_all x1, blocking collectives, several_exchanges(): lax.all_to_all(section, axis, split_axis=0, concat_axis=0, tiled=True)  24.3 us
    all_to_all x1, waiting for transfers between devices, several_exchanges(): lax.all_to_all(section, axis, split_axis=0, concat_axis=0, tiled=True)  18 us
    reduce_sum x4, other arithmetic, one_block(): totals = jnp.sum(jnp.exp(stored - highest[..., None]), axis=-1)  18 us
    another operation x8, local copies, waits for them, and re-layouts  17.3 us
  transfers between devices with their start and end apart: 3, of which 2 were waited for; matrix products, arithmetic and copies ran while one was open for 47% of the time, Pallas kernels for 0%

commit v1 on v0

v1 whole, which is shorter than its diff:
```python
import functools

import jax
import jax.numpy as jnp
import numpy as np
from jax import lax
from jax.experimental import pallas as pl
from jax.experimental.pallas import tpu as pltpu
from jax.sharding import PartitionSpec as P

EPSILON = 1e-06
OUT_SCALE = 0.8
LOG2E = 1.4426950408889634
NEG = -1e30
MESH = pl.DeviceIdType.MESH
CHUNK = 4


def rope_tables(blocks, block, head):
    half = head // 2
    lane = np.arange(2 * head) % head
    inverse = 10000.0 ** (-(lane % half).astype(np.float64) / half)
    sign = np.where(lane < half, -1.0, 1.0)

    def pair(positions):
        angle = positions[:, None] * inverse[None, :]
        return np.stack([np.cos(angle), sign * np.sin(angle)]).astype(np.float32)

    return pair(np.arange(blocks) * float(block)), pair(np.arange(block).astype(np.float64))


def kernel(
    n, nd, head,
    q_hbm, k_hbm, v_hbm, w_hbm, qg_ref, kg_ref, lam_ref, hg_ref, base_ref, offs_ref,
    out_ref,
    kraw, qraw, krot, vall, osend, oin, w_all, sc, acc, gains,
    loc_sem, send_sem, recv_sem, wsend, wrecv, psend, precv,
):
    me = lax.axis_index("sp")
    dp = lax.axis_index("dp")
    core = lax.rem(dp, 2)
    partner = dp + 1 - 2 * core
    right, left = lax.rem(dp + 2, nd), lax.rem(dp + nd - 2, nd)
    steps = nd // 4
    tok = out_ref.shape[1]
    depth, width = w_hbm.shape
    lanes = 2 * head

    def peer_of(t):
        d = (t + 1) // 2
        return lax.rem(me + jnp.where(lax.rem(t, 2) == 1, d, n - d), n)

    def barrier():
        sem = pltpu.get_barrier_semaphore()

        def tell(t, c):
            pl.semaphore_signal(sem, inc=1, device_id={"sp": peer_of(t)}, device_id_type=MESH)
            return c

        lax.fori_loop(1, n, tell, 0)
        for d in (right, left, partner):
            pl.semaphore_signal(sem, inc=1, device_id={"dp": d}, device_id_type=MESH)
        pl.semaphore_wait(sem, n + 2)

    def chunk_copy(which, t):
        peer = peer_of(t)
        if which == 3:
            src, dst = osend.at[peer], oin.at[me]
        else:
            hbm = (k_hbm, v_hbm, q_hbm)[which]
            src = hbm.at[0, :, pl.ds(pl.multiple_of(peer * lanes, lanes), lanes)]
            if which == 1:
                dst = vall.at[pl.ds(pl.multiple_of(me * tok, tok), tok), :]
            else:
                dst = (kraw if which == 0 else qraw).at[me]
        return pltpu.make_async_remote_copy(
            src_ref=src, dst_ref=dst,
            send_sem=send_sem.at[which, t], recv_sem=recv_sem.at[which, me],
            device_id={"sp": peer}, device_id_type=MESH,
        )

    def chunk_arrived(which, t):
        peer = peer_of(t)
        if which == 1:
            dst = vall.at[pl.ds(pl.multiple_of(peer * tok, tok), tok), :]
        else:
            dst = (kraw, None, qraw, oin)[which].at[peer]
        pltpu.make_async_remote_copy(
            src_ref=dst, dst_ref=dst,
            send_sem=send_sem.at[which, t], recv_sem=recv_sem.at[which, peer],
            device_id={"sp": peer}, device_id_type=MESH,
        ).wait_recv()

    def start_all(which):
        def go(t, c):
            chunk_copy(which, t).start()
            return c

        lax.fori_loop(1, n, go, 0)

    def start_far(which):
        def go(s, c):
            chunk_copy(which, n - s).start()
            return c

        lax.fori_loop(1, n, go, 0)

    def own(which):
        cols = pl.ds(pl.multiple_of(me * lanes, lanes), lanes)
        hbm = (k_hbm, v_hbm, q_hbm)[which]
        if which == 1:
            dst = vall.at[pl.ds(pl.multiple_of(me * tok, tok), tok), :]
        else:
            dst = (kraw if which == 0 else qraw).at[me]
        return pltpu.make_async_copy(hbm.at[0, :, cols], dst, loc_sem.at[which])

    def w_at(owner, lo=0, rows=None):
        rows = depth if rows is None else rows
        return w_all.at[pl.ds(lo, rows), pl.ds(pl.multiple_of(owner * width, width), width)]

    half = depth // 2

    def w_copy(step, way):
        back = 2 * (step - 1)
        owner = lax.rem(dp + (nd - back if way == 0 else back), nd)
        if step < steps:
            lo, rows = 0, depth
        else:
            lo, rows = (0, half) if way == 0 else (half, half)
        dst = w_at(owner, lo, rows)
        src = w_hbm.at[pl.ds(lo, rows), :] if step == 1 else dst
        return pltpu.make_async_remote_copy(
            src_ref=src, dst_ref=dst,
            send_sem=wsend.at[step - 1, way], recv_sem=wrecv.at[step - 1, way],
            device_id={"dp": right if way == 0 else left}, device_id_type=MESH,
        )

    def w_arrived(step, way):
        ahead = 2 * step
        owner = lax.rem(dp + (nd - ahead if way == 0 else ahead), nd)
        if step < steps:
            lo, rows = 0, depth
        else:
            lo, rows = (0, half) if way == 0 else (half, half)
        dst = w_at(owner, lo, rows)
        pltpu.make_async_remote_copy(
            src_ref=dst, dst_ref=dst,
            send_sem=wsend.at[step - 1, way], recv_sem=wrecv.at[step - 1, way],
            device_id={"dp": right}, device_id_type=MESH,
        ).wait_recv()

    def p_copy(step, way):
        ahead = 2 * step
        owner = lax.rem(dp + (nd - ahead if way == 0 else ahead), nd)
        dst = w_at(owner)
        return pltpu.make_async_remote_copy(
            src_ref=w_hbm if step == 0 else dst, dst_ref=dst,
            send_sem=psend.at[step, way], recv_sem=precv.at[step, way],
            device_id={"dp": partner}, device_id_type=MESH,
        )

    def p_arrived(step, way):
        ahead = 2 * step
        owner = lax.rem(partner + (nd - ahead if way == 0 else ahead), nd)
        dst = w_at(owner)
        pltpu.make_async_remote_copy(
            src_ref=dst, dst_ref=dst,
            send_sem=psend.at[step, way], recv_sem=precv.at[step, way],
            device_id={"dp": partner}, device_id_type=MESH,
        ).wait_recv()

    p_list = [(0, 0)] + [(s, w) for s in range(1, steps) for w in (0, 1)] + [(steps, 0)]

    def w_step(step):
        for way in (0, 1):
            w_arrived(step, way)
        if step < steps:
            for way in (0, 1):
                w_copy(step + 1, way).start()
                p_copy(step, way).start()
        else:
            p_copy(step, 0).start()

    for which in range(3):
        own(which).start()
    own_w = pltpu.make_async_copy(w_hbm, w_at(dp), loc_sem.at[3])
    own_w.start()
    barrier()
    start_all(0)
    for way in (0, 1):
        w_copy(1, way).start()
    p_copy(0, 0).start()
    start_all(1)

    for row, ref in ((0, qg_ref), (1, kg_ref)):
        g = ref[...]
        gains[row : row + 1, :] = jnp.concatenate([g, g], axis=1)
    lane = lax.broadcasted_iota(jnp.int32, (1, lanes), 1)
    low_half = lax.rem(lane, head) < head // 2
    first_map = lane < head
    ri = lax.broadcasted_iota(jnp.int32, (lanes, lanes), 0) // head
    ci = lax.broadcasted_iota(jnp.int32, (lanes, lanes), 1) // head
    ones = (ri == ci).astype(jnp.float32).astype(jnp.bfloat16)
    acc[...] = jnp.zeros_like(acc)

    def rotate(raw, number, gain):
        x = raw.astype(jnp.float32)
        sq = x * x
        hi = sq.astype(jnp.bfloat16)
        lo = (sq - hi.astype(jnp.float32)).astype(jnp.bfloat16)
        total = jnp.dot(hi, ones, preferred_element_type=jnp.float32) + jnp.dot(
            lo, ones, preferred_element_type=jnp.float32
        )
        y = x * lax.rsqrt(total * (1.0 / head) + EPSILON) * gain
        cb, sb = base_ref[0, pl.ds(number, 1), :], base_ref[1, pl.ds(number, 1), :]
        co, so = offs_ref[0], offs_ref[1]
        cosine = cb * co - sb * so
        sine = sb * co + cb * so
        other = jnp.where(
            low_half, pltpu.roll(y, lanes - head // 2, 1), pltpu.roll(y, head // 2, 1)
        )
        return (y * cosine + other * sine).astype(jnp.bfloat16)

    own(0).wait()

    def key_block(t, c):
        @pl.when(t > 0)
        def _():
            chunk_arrived(0, t)

        number = peer_of(t)
        krot[pl.ds(pl.multiple_of(number * tok, tok), tok), :] = rotate(
            kraw[number], number, gains[1:2, :]
        )
        return c

    lax.fori_loop(0, n, key_block, 0)
    start_far(2)
    w_step(1)

    own(1).wait()
    own(2).wait()
    own_w.wait()

    def value_block(t, c):
        chunk_arrived(1, t)
        return c

    mid = (3 * n) // 4
    lax.fori_loop(1, mid, value_block, 0)
    if steps >= 2:
        w_step(2)
    lax.fori_loop(mid, n, value_block, 0)
    for s in range(3, steps + 1):
        w_step(s)

    lam = lam_ref[me]
    span = CHUNK * tok

    def attend(number):
        q = rotate(qraw[number], number, gains[0:1, :]) * jnp.bfloat16(head**-0.5)
        zero = jnp.zeros_like(q)
        both = jnp.concatenate(
            [jnp.where(first_map, q, zero), jnp.where(first_map, zero, q)], axis=0
        )
        full = number // CHUNK

        def score(j):
            keys = krot[pl.ds(pl.multiple_of(j * span, span), span), :]
            return lax.dot_general(
                both, keys, (((1,), (1,)), ((), ())), preferred_element_type=jnp.float32
            )

        def highest(s, m):
            for c in range(CHUNK):
                m = jnp.maximum(m, s[:, c * tok : (c + 1) * tok])
            return m

        def body(j, m):
            s = score(j)
            sc[j] = s
            return highest(s, m)

        m = lax.fori_loop(0, full, body, jnp.full((2 * tok, tok), NEG, jnp.float32))
        s = score(full)
        row = lax.rem(lax.broadcasted_iota(jnp.int32, s.shape, 0), tok) + number * tok
        col = lax.broadcasted_iota(jnp.int32, s.shape, 1) + full * span
        s = jnp.where(col <= row, s, NEG)
        sc[full] = s
        m = jnp.max(highest(s, m), axis=-1, keepdims=True)

        def expo(j, total):
            e = jnp.exp2((sc[j] - m) * LOG2E)
            sc[j] = e
            for c in range(CHUNK):
                total = total + e[:, c * tok : (c + 1) * tok]
            return total

        total = lax.fori_loop(0, full + 1, expo, jnp.zeros((2 * tok, tok), jnp.float32))
        total = 1.0 / jnp.sum(total, axis=-1, keepdims=True)
        one, two = total[:tok], total[tok:] * lam

        def mix(j, o):
            p = (sc[j, :tok, :] * one - sc[j, tok:, :] * two).astype(jnp.bfloat16)
            return o + jnp.dot(
                p, vall[pl.ds(pl.multiple_of(j * span, span), span), :],
                preferred_element_type=jnp.float32,
            )

        o = lax.fori_loop(0, full + 1, mix, jnp.zeros((tok, vall.shape[1]), jnp.float32))
        o = o * lax.rsqrt(jnp.mean(o * o, axis=-1, keepdims=True) + EPSILON)
        return (o * hg_ref[...] * OUT_SCALE).astype(jnp.bfloat16)

    def query_block(s, c):
        t = n - 1 - s
        number = peer_of(t)

        @pl.when(t > 0)
        def _():
            chunk_arrived(2, t)

        osend[number] = attend(number)

        @pl.when(t > 0)
        def _():
            chunk_copy(3, t).start()

        return c

    lax.fori_loop(0, n, query_block, 0)

    for step, way in p_list:
        p_arrived(step, way)

    def project(block, src):
        rows = pl.ds(pl.multiple_of(block * tok, tok), tok)
        acc[...] += jnp.dot(src, w_all[rows, :], preferred_element_type=jnp.float32)

    project(me, osend[me])

    def head_block(s, c):
        t = n - s
        chunk_arrived(3, t)
        block = peer_of(t)
        project(block, oin[block])
        return c

    lax.fori_loop(1, n, head_block, 0)
    out_ref[0] = acc[...].astype(jnp.bfloat16)

    def sent(t, c):
        for which in range(4):
            chunk_copy(which, t).wait_send()
        return c

    lax.fori_loop(1, n, sent, 0)
    for step in range(1, steps + 1):
        for way in (0, 1):
            w_copy(step, way).wait_send()
    for step, way in p_list:
        p_copy(step, way).wait_send()


def local(query_rows, key_rows, value_rows, query_gain, key_gain, lambdas, head_gain, out_weight):
    n, nd = lax.axis_size("sp"), lax.axis_size("dp")
    head, vdim = query_gain.shape[0], head_gain.shape[0]
    _, tok, total = query_rows.shape
    lanes = 2 * head
    assert lambdas.shape[0] == n and total == n * lanes and vdim == lanes and tok == vdim
    base, offs = rope_tables(n, tok, head)
    columns = out_weight.shape[1] * nd
    steps = nd // 4
    anywhere = pl.BlockSpec(memory_space=pl.ANY)
    vmem = pl.BlockSpec(memory_space=pltpu.VMEM)
    smem = pl.BlockSpec(memory_space=pltpu.SMEM)
    dma = pltpu.SemaphoreType.DMA
    bf16, f32 = jnp.bfloat16, jnp.float32
    return pl.pallas_call(
        functools.partial(kernel, n, nd, head),
        out_shape=jax.ShapeDtypeStruct((1, tok, columns), bf16),
        in_specs=[anywhere] * 4 + [vmem, vmem, smem, vmem, vmem, vmem],
        out_specs=vmem,
        scratch_shapes=[
            pltpu.VMEM((n, tok, lanes), bf16),
            pltpu.VMEM((n, tok, lanes), bf16),
            pltpu.VMEM((n * tok, lanes), bf16),
            pltpu.VMEM((n * tok, vdim), bf16),
            pltpu.VMEM((n, tok, vdim), bf16),
            pltpu.VMEM((n, tok, vdim), bf16),
            pltpu.VMEM((n * vdim, columns), bf16),
            pltpu.VMEM((n // CHUNK, 2 * tok, CHUNK * tok), f32),
            pltpu.VMEM((tok, columns), f32),
            pltpu.VMEM((8, lanes), f32),
            dma((4,)), dma((4, n)), dma((4, n)),
            dma((steps, 2)), dma((steps, 2)), dma((steps + 1, 2)), dma((steps + 1, 2)),
        ],
        compiler_params=pltpu.CompilerParams(
            collective_id=0, has_side_effects=True, vmem_limit_bytes=40 * 2**20
        ),
    )(
        query_rows, key_rows, value_rows, out_weight,
        query_gain.reshape(1, head), key_gain.reshape(1, head), lambdas,
        head_gain.reshape(1, vdim), jnp.asarray(base), jnp.asarray(offs),
    )


def solution(mesh):
    placed = (
        P(("grp", "dp"), "sp", None),
        P(("grp", "dp"), "sp", None),
        P(("grp", "dp"), "sp", None),
        P(),
        P(),
        P(),
        P(),
        P(None, "dp"),
    )
    return jax.shard_map(
        local, mesh=mesh, in_specs=placed, out_specs=P(("grp", "dp"), "sp", None), check_vma=False
    )
```

time: 365 us -> 154 us (0.42)
  the two profiles are of different devices: /device:TPU:82 before, /device:TPU:80 now
where the time goes in v1:
time: 154 us
  Pallas kernels  146 us (95%)
  local copies, waits for them, and re-layouts  7.27 us (5%)
    pallas_call x1, Pallas kernels, local(): pl.pallas_call(functools.partial(kernel, n, nd, head), out_shape=jax.Shap...  146 us
    unnamed x21, local copies, waits for them, and re-layouts  7.27 us

profile of v1, /device:TPU:80, one launch (start us, length us, event | category | flops | bytes accessed | tf_op | source)
XLA Modules:
  0.0 153.6 jit_solution(6150748701924957491)
XLA Ops:
  0.0 0.0 copy-start.9
  0.0 0.0 copy-start.6
  0.0 0.0 copy-start.7
  0.0 0.0 copy-start.8
  0.0 0.6 copy-done.9
  0.7 0.0 copy-done.6
  0.7 0.0 copy-done.7
  0.7 0.0 copy-done.8
  0.7 0.0 copy-start
  0.7 1.0 copy-done
  1.7 0.0 copy-start.1
  1.7 1.0 copy-done.1
  2.8 0.0 copy-start.2
  2.8 1.0 copy-done.2
  3.8 0.0 copy-start.3
  3.8 1.0 copy-done.3
  4.9 0.0 copy-start.4
  4.9 0.9 copy-done.4
  5.8 0.0 copy-start.5
  5.8 0.7 copy-done.5
  6.5 146.3 %shard_map.100 = bf16[1,128,2048]{2,1,0:T(8,128)(2,1)S(1)} custom-call(bf16[1,128,2048]{2,1,0:T(8,128)(2,1)S(1)} %copy-done, bf16[1,128,2048]{2,1,0:T(8,128)(2,1)S(1)} %copy-done.1, bf16[1,128,2048]{2,1,0:T(8,128)(2,1)S(1)} %copy-done.2, bf16[2048,128]{1,0:T(8,128)(2,1)S(1)} %copy-done.3, f32[1,64]{1,0:T(1,128)S(1)} %bitcast.3, f32[1,64]{1,0:T(1,128)S(1)} %bitcast.4, ...), custom_call_target="tpu_custom_call" | custom-call | tf_op jit(solution)/shard_map/pallas_call | solution.py:378
  152.8 0.8 copy.12
Async XLA Ops:
  0.0 0.7 copy-start.9
  0.0 0.7 copy-start.6
  0.0 0.7 copy-start.7
  0.0 0.7 copy-start.8
  0.7 1.0 copy-start
  1.7 1.0 copy-start.1
  2.8 1.0 copy-start.2
  3.8 1.0 copy-start.3
  4.9 0.9 copy-start.4
  5.8 0.7 copy-start.5

commit v2 on v1

v2 whole, which is shorter than its diff:
```python
import functools

import jax
import jax.numpy as jnp
import numpy as np
from jax import lax
from jax.experimental import pallas as pl
from jax.experimental.pallas import tpu as pltpu
from jax.sharding import PartitionSpec as P

EPSILON = 1e-06
OUT_SCALE = 0.8
LOG2E = 1.4426950408889634
NEG = -1e30
MESH = pl.DeviceIdType.MESH
CHUNK = 4


def rope_tables(blocks, block, head):
    half = head // 2
    lane = np.arange(2 * head) % head
    inverse = 10000.0 ** (-(lane % half).astype(np.float64) / half)
    sign = np.where(lane < half, -1.0, 1.0)

    def pair(positions):
        angle = positions[:, None] * inverse[None, :]
        return np.stack([np.cos(angle), sign * np.sin(angle)]).astype(np.float32)

    return np.concatenate(
        [pair(np.arange(blocks) * float(block)), pair(np.arange(block).astype(np.float64))], axis=1
    )


def kernel(
    n, nd, head,
    q_hbm, k_hbm, v_hbm, w_hbm, qg_ref, kg_ref, lam_ref, hg_ref, table_ref,
    out_ref,
    kraw, vraw, qraw, krot, vall, osend, oin, w_all, sc, acc, gains,
    loc_sem, send_sem, recv_sem, wsend, wrecv, psend, precv, ready, lead_in,
):
    me = lax.axis_index("sp")
    dp = lax.axis_index("dp")
    lead_ring = (dp == 0) & (lax.axis_index("grp") == 0)
    lead_plane = (me == 0) & (lax.axis_index("grp") == 0)
    is_lead = lead_ring & lead_plane
    core = lax.rem(dp, 2)
    partner = dp + 1 - 2 * core
    reach = max(nd // 8, 1)
    along = [
        (k, way, lax.rem(dp + (2 * k if way == 0 else nd - 2 * k), nd))
        for k in range(1, reach + 1)
        for way in (0, 1)
    ]
    beside = [d for _, _, d in along] + [partner]
    tok = out_ref.shape[1]
    depth, width = w_hbm.shape
    lanes = 2 * head

    first = jnp.where(lead_ring, 1, 0)
    pos = lax.rem(me - first + n, n)

    def at(p):
        return lax.rem(p + first, n)

    def leads(d):
        return lead_plane & (d == 0)

    beside_lead = sum(leads(d).astype(jnp.int32) for d in beside)

    def enter():
        sem = pltpu.get_barrier_semaphore()

        @pl.when(jnp.logical_not(is_lead))
        def _():
            for d in beside:
                pl.semaphore_signal(sem, inc=1, device_id={"dp": d}, device_id_type=MESH)

        pl.semaphore_wait(sem, len(beside) - beside_lead + jnp.where(pos > 0, 1, 0))

        @pl.when(pos < n - 1)
        def _():
            pl.semaphore_signal(sem, inc=1, device_id={"sp": at(pos + 1)}, device_id_type=MESH)

        @pl.when(is_lead)
        def _():
            for d in beside:
                pl.semaphore_signal(lead_in, inc=1, device_id={"dp": d}, device_id_type=MESH)

        def tell(p, c):
            pl.semaphore_signal(ready.at[me], inc=1, device_id={"sp": at(p)}, device_id_type=MESH)
            return c

        lax.fori_loop(0, pos, tell, 0)

    raws = (kraw, vraw, qraw)

    def chunk_copy(which, peer):
        if which == 3:
            src = osend.at[peer]
            dst = oin.at[:, pl.ds(pl.multiple_of(me * tok, tok), tok)]
        else:
            src = (k_hbm, v_hbm, q_hbm)[which].at[
                0, :, pl.ds(pl.multiple_of(peer * lanes, lanes), lanes)
            ]
            dst = raws[which].at[me]
        return pltpu.make_async_remote_copy(
            src_ref=src, dst_ref=dst,
            send_sem=send_sem.at[which, peer], recv_sem=recv_sem.at[which, me],
            device_id={"sp": peer}, device_id_type=MESH,
        )

    def chunk_arrived(which, peer):
        if which == 3:
            dst = oin.at[:, pl.ds(pl.multiple_of(peer * tok, tok), tok)]
        else:
            dst = raws[which].at[peer]
        pltpu.make_async_remote_copy(
            src_ref=dst, dst_ref=dst,
            send_sem=send_sem.at[which, peer], recv_sem=recv_sem.at[which, peer],
            device_id={"sp": peer}, device_id_type=MESH,
        ).wait_recv()

    def own(which):
        cols = pl.ds(pl.multiple_of(me * lanes, lanes), lanes)
        return pltpu.make_async_copy(
            (k_hbm, v_hbm, q_hbm)[which].at[0, :, cols], raws[which].at[me], loc_sem.at[which]
        )

    def w_at(owner, lo=0, rows=None):
        rows = depth if rows is None else rows
        return w_all.at[pl.ds(lo, rows), pl.ds(pl.multiple_of(owner * width, width), width)]

    half = depth // 2

    def away(device, chips, way):
        return lax.rem(device + (nd - 2 * chips if way == 0 else 2 * chips), nd)

    def remote(src, dst, send, recv, d):
        return pltpu.make_async_remote_copy(
            src_ref=src, dst_ref=dst, send_sem=send, recv_sem=recv,
            device_id={"dp": d}, device_id_type=MESH,
        )

    def w_part(phase, k, way):
        if phase == 0 or k < reach:
            return 0, depth
        return (0, half) if way == 0 else (half, half)

    def w_copy(phase, k, way, d):
        dst = w_at(away(dp, phase * k, way), *w_part(phase, k, way))
        i = phase * reach + k - 1
        return remote(w_hbm if phase == 0 else dst, dst, wsend.at[i, way], wrecv.at[i, way], d)

    def w_arrived(phase, k, way):
        dst = w_at(away(dp, k + phase * reach, way), *w_part(phase, k, way))
        i = phase * reach + k - 1
        remote(dst, dst, wsend.at[i, way], wrecv.at[i, way], partner).wait_recv()

    p_list = [(0, 0)] + [(c, way) for c in range(1, 2 * reach) for way in (0, 1)] + [(2 * reach, 0)]

    def p_copy(chips, way):
        dst = w_at(away(dp, chips, way))
        return remote(
            w_hbm if chips == 0 else dst, dst, psend.at[chips, way], precv.at[chips, way], partner
        )

    def p_arrived(chips, way):
        dst = w_at(away(partner, chips, way))
        remote(dst, dst, psend.at[chips, way], precv.at[chips, way], partner).wait_recv()

    def w_first(to_lead):
        copies = [(w_copy(0, k, way, d), d) for k, way, d in along] + [(p_copy(0, 0), partner)]
        for copy, d in copies:

            @pl.when(leads(d) if to_lead else jnp.logical_not(leads(d)))
            def _():
                copy.start()

    far = [d for k, _, d in along if k == reach]

    def w_on():
        for k in range(1, reach + 1):
            for way in (0, 1):
                w_arrived(0, k, way)
                w_copy(1, k, way, far[way]).start()
                p_copy(k, way).start()

    def w_rest():
        for k in range(1, reach + 1):
            for way in (0, 1):
                w_arrived(1, k, way)
                if k < reach:
                    p_copy(reach + k, way).start()
        p_copy(2 * reach, 0).start()

    for which in range(3):
        own(which).start()
    own_w = pltpu.make_async_copy(w_hbm, w_at(dp), loc_sem.at[3])
    own_w.start()
    enter()

    def send_to(p):
        for which in range(3):
            chunk_copy(which, at(p)).start()

    def send_lower(s, c):
        send_to(pos - 1 - s)
        return c

    def send_upper(p, c):
        pl.semaphore_wait(ready.at[at(p)], 1)
        send_to(p)
        return c

    w_first(False)
    lax.fori_loop(0, pos, send_lower, 0)
    lax.fori_loop(pos + 1, n, send_upper, 0)

    @pl.when(jnp.logical_not(is_lead) & (beside_lead > 0))
    def _():
        pl.semaphore_wait(lead_in, beside_lead)
        w_first(True)


    for row, ref in ((0, qg_ref), (1, kg_ref)):
        g = ref[...]
        gains[row : row + 1, :] = jnp.concatenate([g, g], axis=1)
    lane = lax.broadcasted_iota(jnp.int32, (1, lanes), 1)
    low_half = lax.rem(lane, head) < head // 2
    first_map = lane < head
    ri = lax.broadcasted_iota(jnp.int32, (lanes, lanes), 0) // head
    ci = lax.broadcasted_iota(jnp.int32, (lanes, lanes), 1) // head
    ones = (ri == ci).astype(jnp.float32).astype(jnp.bfloat16)
    krot[...] = jnp.zeros_like(krot)
    vall[...] = jnp.zeros_like(vall)

    def rotate(raw, number, gain):
        x = raw.astype(jnp.float32)
        sq = x * x
        hi = sq.astype(jnp.bfloat16)
        lo = (sq - hi.astype(jnp.float32)).astype(jnp.bfloat16)
        total = jnp.dot(hi, ones, preferred_element_type=jnp.float32) + jnp.dot(
            lo, ones, preferred_element_type=jnp.float32
        )
        y = x * lax.rsqrt(total * (1.0 / head) + EPSILON) * gain
        cb, sb = table_ref[0, pl.ds(number, 1), :], table_ref[1, pl.ds(number, 1), :]
        co, so = table_ref[0, n : n + tok, :], table_ref[1, n : n + tok, :]
        cosine = cb * co - sb * so
        sine = sb * co + cb * so
        other = jnp.where(
            low_half, pltpu.roll(y, lanes - head // 2, 1), pltpu.roll(y, head // 2, 1)
        )
        return (y * cosine + other * sine).astype(jnp.bfloat16)

    lam = lam_ref[me]
    span = CHUNK * tok

    def attend(number):
        q = rotate(qraw[number], number, gains[0:1, :]) * jnp.bfloat16(head**-0.5)
        zero = jnp.zeros_like(q)
        both = jnp.concatenate(
            [jnp.where(first_map, q, zero), jnp.where(first_map, zero, q)], axis=0
        )
        full = number // CHUNK

        def score(j):
            keys = krot[pl.ds(pl.multiple_of(j * span, span), span), :]
            return lax.dot_general(
                both, keys, (((1,), (1,)), ((), ())), preferred_element_type=jnp.float32
            )

        def highest(s, m):
            for c in range(CHUNK):
                m = jnp.maximum(m, s[:, c * tok : (c + 1) * tok])
            return m

        def body(j, m):
            s = score(j)
            sc[j] = s
            return highest(s, m)

        m = lax.fori_loop(0, full, body, jnp.full((2 * tok, tok), NEG, jnp.float32))
        s = score(full)
        row = lax.rem(lax.broadcasted_iota(jnp.int32, s.shape, 0), tok) + number * tok
        col = lax.broadcasted_iota(jnp.int32, s.shape, 1) + full * span
        s = jnp.where(col <= row, s, NEG)
        sc[full] = s
        m = jnp.max(highest(s, m), axis=-1, keepdims=True)

        def expo(j, total):
            e = jnp.exp2((sc[j] - m) * LOG2E)
            sc[j] = e
            for c in range(CHUNK):
                total = total + e[:, c * tok : (c + 1) * tok]
            return total

        total = lax.fori_loop(0, full + 1, expo, jnp.zeros((2 * tok, tok), jnp.float32))
        total = 1.0 / jnp.sum(total, axis=-1, keepdims=True)
        one, two = total[:tok], total[tok:] * lam

        def mix(j, o):
            p = (sc[j, :tok, :] * one - sc[j, tok:, :] * two).astype(jnp.bfloat16)
            return o + jnp.dot(
                p, vall[pl.ds(pl.multiple_of(j * span, span), span), :],
                preferred_element_type=jnp.float32,
            )

        o = lax.fori_loop(0, full + 1, mix, jnp.zeros((tok, vall.shape[1]), jnp.float32))
        o = o * lax.rsqrt(jnp.mean(o * o, axis=-1, keepdims=True) + EPSILON)
        return (o * hg_ref[...] * OUT_SCALE).astype(jnp.bfloat16)

    for which in range(3):
        own(which).wait()

    w_on_turn = jnp.where(is_lead, n // 16, (3 * n) // 8)
    w_rest_turn = jnp.where(is_lead, n // 2, jnp.where(me < n // 2, (3 * n) // 4, n - 1))

    def turn(s, c):
        @pl.when(s == w_on_turn)
        def _():
            w_on()

        @pl.when(s == w_rest_turn)
        def _():
            w_rest()

        number = s

        @pl.when(number != me)
        def _():
            for which in range(3):
                chunk_arrived(which, number)

        rows = pl.ds(pl.multiple_of(number * tok, tok), tok)
        krot[rows, :] = rotate(kraw[number], number, gains[1:2, :])
        vall[rows, :] = vraw[number]

        o = attend(number)

        @pl.when(number == me)
        def _():
            oin[:, pl.ds(pl.multiple_of(me * tok, tok), tok)] = o

        @pl.when(number != me)
        def _():
            osend[number] = o
            chunk_copy(3, number).start()

        return c

    lax.fori_loop(0, n, turn, 0)
    own_w.wait()
    for chips, way in p_list:
        p_arrived(chips, way)

    acc[...] = jnp.zeros_like(acc)
    groups = n // CHUNK

    def head_group(turn, c):
        g = lax.rem(turn + first, groups)
        for j in range(CHUNK):
            block = g * CHUNK + j

            @pl.when(block != me)
            def _():
                chunk_arrived(3, block)

        cols = pl.ds(pl.multiple_of(g * span, span), span)
        acc[...] += jnp.dot(oin[:, cols], w_all[cols, :], preferred_element_type=jnp.float32)
        return c

    lax.fori_loop(0, groups, head_group, 0)
    out_ref[0] = acc[...].astype(jnp.bfloat16)

    def sent(p, c):
        @pl.when(p != me)
        def _():
            for which in range(4):
                chunk_copy(which, p).wait_send()

        return c

    lax.fori_loop(0, n, sent, 0)
    for phase in (0, 1):
        for k, way, d in along:
            w_copy(phase, k, way, d).wait_send()
    for chips, way in p_list:
        p_copy(chips, way).wait_send()


def local(query_rows, key_rows, value_rows, query_gain, key_gain, lambdas, head_gain, out_weight):
    n, nd = lax.axis_size("sp"), lax.axis_size("dp")
    head, vdim = query_gain.shape[0], head_gain.shape[0]
    _, tok, total = query_rows.shape
    lanes = 2 * head
    assert lambdas.shape[0] == n and total == n * lanes and vdim == lanes and tok == vdim
    table = rope_tables(n, tok, head)
    columns = out_weight.shape[1] * nd
    reach = max(nd // 8, 1)
    anywhere = pl.BlockSpec(memory_space=pl.ANY)
    vmem = pl.BlockSpec(memory_space=pltpu.VMEM)
    smem = pl.BlockSpec(memory_space=pltpu.SMEM)
    dma = pltpu.SemaphoreType.DMA
    bf16, f32 = jnp.bfloat16, jnp.float32
    return pl.pallas_call(
        functools.partial(kernel, n, nd, head),
        out_shape=jax.ShapeDtypeStruct((1, tok, columns), bf16),
        in_specs=[anywhere] * 4 + [vmem, vmem, smem, vmem, vmem],
        out_specs=vmem,
        scratch_shapes=[
            pltpu.VMEM((n, tok, lanes), bf16),
            pltpu.VMEM((n, tok, vdim), bf16),
            pltpu.VMEM((n, tok, lanes), bf16),
            pltpu.VMEM((n * tok, lanes), bf16),
            pltpu.VMEM((n * tok, vdim), bf16),
            pltpu.VMEM((n, tok, vdim), bf16),
            pltpu.VMEM((tok, n * vdim), bf16),
            pltpu.VMEM((n * vdim, columns), bf16),
            pltpu.VMEM((n // CHUNK, 2 * tok, CHUNK * tok), f32),
            pltpu.VMEM((tok, columns), f32),
            pltpu.VMEM((8, lanes), f32),
            dma((4,)), dma((4, n)), dma((4, n)),
            dma((2 * reach, 2)), dma((2 * reach, 2)),
            dma((2 * reach + 1, 2)), dma((2 * reach + 1, 2)),
            pltpu.SemaphoreType.REGULAR((n,)), pltpu.SemaphoreType.REGULAR,
        ],
        compiler_params=pltpu.CompilerParams(
            collective_id=0, has_side_effects=True, vmem_limit_bytes=67_043_328
        ),
    )(
        query_rows, key_rows, value_rows, out_weight,
        query_gain.reshape(1, head), key_gain.reshape(1, head), lambdas,
        head_gain.reshape(1, vdim), jnp.asarray(table),
    )


def solution(mesh):
    placed = (
        P(("grp", "dp"), "sp", None),
        P(("grp", "dp"), "sp", None),
        P(("grp", "dp"), "sp", None),
        P(),
        P(),
        P(),
        P(),
        P(None, "dp"),
    )
    return jax.shard_map(
        local, mesh=mesh, in_specs=placed, out_specs=P(("grp", "dp"), "sp", None), check_vma=False
    )
```

time: 154 us -> 141 us (0.916)
  the two profiles are of different devices: /device:TPU:80 before, /device:TPU:192 now
where the time goes in v2:
time: 141 us
  Pallas kernels  139 us (99%)
  local copies, waits for them, and re-layouts  1.88 us (1%)
    pallas_call x1, Pallas kernels, local(): pl.pallas_call(functools.partial(kernel, n, nd, head), out_shape=jax.Shap...  139 us

profile of v2, /device:TPU:192, one launch (start us, length us, event | category | flops | bytes accessed | tf_op | source)
XLA Modules:
  0.0 141.0 jit_solution(12589140142286051636)
XLA Ops:
  0.0 139.1 %shard_map.91 = bf16[1,128,2048]{2,1,0:T(8,128)(2,1)} custom-call(bf16[1,128,2048]{2,1,0:T(8,128)(2,1)} %q_hbm.1, bf16[1,128,2048]{2,1,0:T(8,128)(2,1)} %k_hbm.1, bf16[1,128,2048]{2,1,0:T(8,128)(2,1)} %v_hbm.1, bf16[2048,128]{1,0:T(8,128)(2,1)} %w_hbm.1, f32[1,64]{1,0:T(1,128)} %bitcast.3, f32[1,64]{1,0:T(1,128)} %bitcast.4, f32[16]{0:T(128)} %lam_ref.1, ...), custom_call_target="tpu_custom_call" | custom-call | tf_op jit(solution)/shard_map/pallas_call | solution.py:405
  139.1 1.9 %copy.11 = bf16[1,128,2048]{2,1,0:T(8,128)(2,1)} copy(bf16[1,128,2048]{2,1,0:T(8,128)(2,1)} %shard_map.91) | data formatting | bytes 1048576

commit v3 on v2

--- a/solution.py
+++ b/solution.py
@@ -204,7 +204,9 @@
             chunk_copy(which, at(p)).start()
 
     def send_lower(s, c):
-        send_to(pos - 1 - s)
+        k = s // 2
+        both_ways = jnp.where(lax.rem(s, 2) == 0, pos - 1 - k, k)
+        send_to(jnp.where(pos > n // 2, both_ways, pos - 1 - s))
         return c
 
     def send_upper(p, c):

time: 141 us -> 135 us (0.957)
  Pallas kernels: 139 us -> 133 us
    pallas_call x1, Pallas kernels: 139 us -> 133 us  [local(): pl.pallas_call(functools.partial(kernel, n, nd, head), out_shape=jax.Shap...]
where the time goes in v3:
time: 135 us
  Pallas kernels  133 us (99%)
  local copies, waits for them, and re-layouts  1.88 us (1%)
    pallas_call x1, Pallas kernels, local(): pl.pallas_call(functools.partial(kernel, n, nd, head), out_shape=jax.Shap...  133 us

profile of v3, /device:TPU:192, one launch (start us, length us, event | category | flops | bytes accessed | tf_op | source)
XLA Modules:
  0.0 134.7 jit_solution(4472764173858575256)
XLA Ops:
  0.0 132.8 %shard_map.91 = bf16[1,128,2048]{2,1,0:T(8,128)(2,1)} custom-call(bf16[1,128,2048]{2,1,0:T(8,128)(2,1)} %q_hbm.1, bf16[1,128,2048]{2,1,0:T(8,128)(2,1)} %k_hbm.1, bf16[1,128,2048]{2,1,0:T(8,128)(2,1)} %v_hbm.1, bf16[2048,128]{1,0:T(8,128)(2,1)} %w_hbm.1, f32[1,64]{1,0:T(1,128)} %bitcast.3, f32[1,64]{1,0:T(1,128)} %bitcast.4, f32[16]{0:T(128)} %lam_ref.1, ...), custom_call_target="tpu_custom_call" | custom-call | tf_op jit(solution)/shard_map/pallas_call | solution.py:407
  132.8 1.9 %copy.11 = bf16[1,128,2048]{2,1,0:T(8,128)(2,1)} copy(bf16[1,128,2048]{2,1,0:T(8,128)(2,1)} %shard_map.91) | data formatting | bytes 1048576

commit v4 on v2

--- a/solution.py
+++ b/solution.py
@@ -203,8 +203,27 @@
         for which in range(3):
             chunk_copy(which, at(p)).start()
 
+    wraps = jnp.maximum(jnp.where(lead_ring & (pos > n // 2), n, pos - n // 2), 0)
+
+    near = (3 * n) // 8
+    holds = (pos > n // 2) & jnp.logical_not(lead_ring)
+
+    def held(p):
+        return holds & (pos - p > near) & (pos - p <= n // 2)
+
+    def send_held(k, c):
+        send_to(pos - k)
+        return c
+
     def send_lower(s, c):
-        send_to(pos - 1 - s)
+        down = jnp.where(s < 2 * wraps, s // 2, s - wraps)
+        turned = (s < 2 * wraps) & (lax.rem(s, 2) == 1)
+        p = jnp.where(turned, s // 2, pos - 1 - down)
+
+        @pl.when(jnp.logical_not(held(p)))
+        def _():
+            send_to(p)
+
         return c
 
     def send_upper(p, c):
@@ -214,7 +233,8 @@
 
     w_first(False)
     lax.fori_loop(0, pos, send_lower, 0)
-    lax.fori_loop(pos + 1, n, send_upper, 0)
+    ahead = jnp.where(lead_ring, (3 * n) // 4 + 1, n)
+    lax.fori_loop(pos + 1, jnp.maximum(pos + 1, ahead), send_upper, 0)
 
     @pl.when(jnp.logical_not(is_lead) & (beside_lead > 0))
     def _():
@@ -312,10 +332,14 @@
     for which in range(3):
         own(which).wait()
 
-    w_on_turn = jnp.where(is_lead, n // 16, (3 * n) // 8)
-    w_rest_turn = jnp.where(is_lead, n // 2, jnp.where(me < n // 2, (3 * n) // 4, n - 1))
+    w_on_turn = jnp.where(is_lead, 0, (3 * n) // 8)
+    w_rest_turn = jnp.where(is_lead, n // 16, jnp.where(me < n // 2, (3 * n) // 4, n - 1))
 
     def turn(s, c):
+        @pl.when((s == n // 8) & holds)
+        def _():
+            lax.fori_loop(near + 1, n // 2 + 1, send_held, 0)
+
         @pl.when(s == w_on_turn)
         def _():
             w_on()
@@ -345,6 +369,12 @@
         def _():
             osend[number] = o
             chunk_copy(3, number).start()
+
+        upper = jnp.maximum(ahead, pos + 1) + s
+
+        @pl.when(upper < n)
+        def _():
+            send_upper(upper, 0)
 
         return c
 

time: 141 us -> 133 us (0.943)
  Pallas kernels: 139 us -> 131 us
    pallas_call x1, Pallas kernels: 139 us -> 131 us  [local(): pl.pallas_call(functools.partial(kernel, n, nd, head), out_shape=jax.Shap...]
where the time goes in v4:
time: 133 us
  Pallas kernels  131 us (98%)
  local copies, waits for them, and re-layouts  1.88 us (1%)
    pallas_call x1, Pallas kernels, local(): pl.pallas_call(functools.partial(kernel, n, nd, head), out_shape=jax.Shap...  131 us

profile of v4, /device:TPU:192, one launch (start us, length us, event | category | flops | bytes accessed | tf_op | source)
XLA Modules:
  0.0 133.3 jit_solution(680694445693753184)
XLA Ops:
  0.0 131.4 %shard_map.91 = bf16[1,128,2048]{2,1,0:T(8,128)(2,1)} custom-call(bf16[1,128,2048]{2,1,0:T(8,128)(2,1)} %q_hbm.1, bf16[1,128,2048]{2,1,0:T(8,128)(2,1)} %k_hbm.1, bf16[1,128,2048]{2,1,0:T(8,128)(2,1)} %v_hbm.1, bf16[2048,128]{1,0:T(8,128)(2,1)} %w_hbm.1, f32[1,64]{1,0:T(1,128)} %bitcast.3, f32[1,64]{1,0:T(1,128)} %bitcast.4, f32[16]{0:T(128)} %lam_ref.1, ...), custom_call_target="tpu_custom_call" | custom-call | tf_op jit(solution)/shard_map/pallas_call | solution.py:435
  131.4 1.9 %copy.11 = bf16[1,128,2048]{2,1,0:T(8,128)(2,1)} copy(bf16[1,128,2048]{2,1,0:T(8,128)(2,1)} %shard_map.91) | data formatting | bytes 1048576
